TPU v7x, 32 devices: a whole 2x2x4 slice. The times are simulated.
32 devices in a mesh: rep: 2 (over x), fs: 8 (over z, y), tp: 2 (over core).
Axes of the slice: x: 2, y: 2, z: 4, core: 2. Of those that a mesh axis runs over, the one named last changes fastest.
Arguments:
- layer_in: bfloat16 [16384, 2048], P(('rep', 'fs'), 'tp'), may hold values from -60 to 60
- mix_gain: bfloat16 [2048], P('tp'), may hold values from 0.099609375 to 1.8984375
- pool_weight: float32 [4, 512, 512], P('tp', None, 'fs'), may hold values from -0.25 to 0.25
- pool_scale: float32 [4, 512], P('tp'), may hold values from 0.1 to 1.9
- out_weight: float32 [2048, 2048], P('tp', 'fs'), may hold values from -0.125 to 0.125
- out_scale: float32 [2048], P('tp'), may hold values from 0.1 to 1.9
- channel_gain: bfloat16 [2048], P('tp'), may hold values from 0.099609375 to 1.8984375
- up_weight: float32 [2048, 2816], P('fs', 'tp'), may hold values from -0.125 to 0.125
- up_scale: float32 [2816], P('tp'), may hold values from 0.1 to 1.9
- gate_weight: float32 [2048, 2816], P('fs', 'tp'), may hold values from -0.125 to 0.125
- gate_scale: float32 [2816], P('tp'), may hold values from 0.1 to 1.9
- conv_weight: float32 [3, 2816], P(None, 'tp'), may hold values from -3 to 3
- down_weight: float32 [2816, 2048], P('tp', 'fs'), may hold values from -0.109375 to 0.109375
- down_scale: float32 [2048], P('tp'), may hold values from 0.1 to 1.9
Outputs:
- layer_out: bfloat16 [16384, 2048], P(('rep', 'fs'), 'tp')
All inputs are finite; a program needn't handle non-finite values.
Results may differ from a plain program's by a relative error of at most 0.0095.
Values may be sent and summed in bfloat16 or wider, within the bound.
A program may use at most 128 MiB of HBM per device.

v0:
```python
import functools

import jax
import jax.numpy as jnp
from jax import lax
from jax.experimental import pallas as pl
from jax.experimental.pallas import tpu as pltpu
from jax.sharding import PartitionSpec as P

LENGTH = 256
EPS = 1e-06
TILE = 16
MESH = pl.DeviceIdType.MESH

ALONG = (0.78, 0.78, 0.78, 0.78, 0.72)
ACROSS = (0.58, 0.58, 0.58, 0.58, 0.60)


class Chunk:
    def __init__(self, index, buffer, shard, offset, rows, along, across):
        units = rows // TILE
        least = (units + 1) // 2
        self.index, self.buffer, self.shard, self.offset, self.rows = index, buffer, shard, offset, rows
        self.along = TILE * min(max(round(units * along), least), units)
        self.across = min(TILE * max(round(units * across), least), self.along)


def dot(left, right):
    return jnp.dot(left, right, preferred_element_type=jnp.float32)


def layer_kernel(n, chunks, *refs):
    x_in, pool_in, out_in, up_in, gate_in, down_in = refs[:6]
    small_in, o_ref, small = refs[6:14], refs[14], refs[15:23]
    poolb, outb, upb, gateb, downb, s_pool, s_out, s_up, s_gate, s_down = refs[23:33]
    xm, keep, sent, recv, cn, lift, ss, ssr = refs[33:41]
    in_sem, zs, zr, ys, yr, xs, xr, ts, tr = refs[41:]
    mix_gain, pool_scale, out_scale, channel_gain, up_scale, gate_scale, conv_weight, down_scale = small
    buffers = (poolb, outb, upb, gateb, downb)

    rows, half = xm.shape
    width = 2 * half
    seqs = rows // LENGTH
    shards = 2 * n
    blocks, _, block = keep.shape
    hidden_width = lift.shape[1]
    group = poolb.shape[1]
    groups = half // group
    pool_rows = pool_in.shape[0]
    lane = pool_rows // groups

    r, f, core = lax.axis_index("rep"), lax.axis_index("fs"), lax.axis_index("tp")
    a, b = f // 2, f % 2

    def order(j):
        near = jnp.minimum(a, n - 1 - a)
        odd = j % 2
        paired = a + (1 - 2 * odd) * ((j + 1) // 2)
        way = jnp.where(a < n - 1 - a, 1, -1)
        return jnp.where(j <= 2 * near, paired, a + way * (j - near))

    def rows_of(chunk, shard, start, count):
        begin = pl.multiple_of(shard * chunk.shard + chunk.offset + start, TILE)
        return buffers[chunk.buffer].at[pl.ds(begin, count)]

    def z_copy(chunk, s, target, slot):
        part = rows_of(chunk, 2 * s + b, r * (chunk.rows - chunk.along), chunk.along)
        return pltpu.make_async_remote_copy(
            src_ref=part, dst_ref=part, send_sem=zs.at[chunk.index, slot], recv_sem=zr.at[chunk.index, s],
            device_id={"fs": 2 * target + b}, device_id_type=MESH,
        )

    def y_copy(chunk, s, side):
        part = rows_of(chunk, 2 * s + side, r * (chunk.rows - chunk.across), chunk.across)
        return pltpu.make_async_remote_copy(
            src_ref=part, dst_ref=part, send_sem=ys.at[chunk.index, s], recv_sem=yr.at[chunk.index, s],
            device_id={"fs": 2 * a + 1 - b}, device_id_type=MESH,
        )

    def x_copy(chunk, s, kind, end):
        had = chunk.across if kind else chunk.along
        part = rows_of(chunk, 2 * s + (1 - b if kind else b), end * had, chunk.rows - had)
        return pltpu.make_async_remote_copy(
            src_ref=part, dst_ref=part, send_sem=xs.at[chunk.index, kind, s], recv_sem=xr.at[chunk.index, kind, s],
            device_id={"rep": 1 - r}, device_id_type=MESH,
        )

    def onward(s):
        target = jnp.where(s < a, a + 1, a - 1)
        return target, (target >= 0) & (target < n)

    def begin(chunk):
        @pl.when(a < n - 1)
        def _():
            z_copy(chunk, a, a + 1, a).start()

        @pl.when(a > 0)
        def _():
            z_copy(chunk, a, a - 1, n).start()

        y_copy(chunk, a, b).start()

    def z_event(chunk, j):
        s = order(j)
        target, valid = onward(s)
        z_copy(chunk, s, a, s).wait_recv()

        @pl.when(valid)
        def _():
            z_copy(chunk, s, target, s).start()

        y_copy(chunk, s, b).start()
        if chunk.rows > chunk.along:
            x_copy(chunk, s, 0, r).start()

    def y_event(chunk, j):
        s = order(j)
        y_copy(chunk, s, 1 - b).wait_recv()
        if chunk.rows > chunk.across:
            x_copy(chunk, s, 1, r).start()

    def x_wait(chunk, j, kind):
        if kind and chunk.rows > chunk.across:
            x_copy(chunk, order(j), 1, 1 - r).wait_recv()
        if not kind and chunk.rows > chunk.along:
            x_copy(chunk, order(j), 0, 1 - r).wait_recv()

    def arrived(which):
        for chunk in which:
            x_wait(chunk, 0, 1)

            def step(j, carry):
                x_wait(chunk, j, 0)
                x_wait(chunk, j, 1)
                return carry

            lax.fori_loop(1, n, step, 0)

    def finish(chunk):
        @pl.when(a < n - 1)
        def _():
            z_copy(chunk, a, a + 1, a).wait_send()

        @pl.when(a > 0)
        def _():
            z_copy(chunk, a, a - 1, n).wait_send()

        def step(j, carry):
            s = order(j)
            target, valid = onward(s)
            y_copy(chunk, s, b).wait_send()
            if chunk.rows > chunk.across:
                x_copy(chunk, s, 1, r).wait_send()

            @pl.when(j > 0)
            def _():
                if chunk.rows > chunk.along:
                    x_copy(chunk, s, 0, r).wait_send()

                @pl.when(valid)
                def _():
                    z_copy(chunk, s, target, s).wait_send()

            return carry

        lax.fori_loop(0, n, step, 0)

    def stage(which, before, piece, count):
        for chunk in which:
            z_event(chunk, 1)
        for chunk in which:
            y_event(chunk, 0)
        before()

        def step(j, carry):
            def one(q, inner):
                piece(q)
                return inner

            lax.fori_loop((j - 1) * count // (n - 1), j * count // (n - 1), one, 0)

            @pl.when(j < n - 1)
            def _():
                for chunk in which:
                    z_event(chunk, j + 1)
                for chunk in which:
                    y_event(chunk, j)

            return carry

        lax.fori_loop(1, n, step, 0)
        for chunk in which:
            y_event(chunk, n - 1)

    def t_copy(kind, index, src, dst):
        return pltpu.make_async_remote_copy(
            src_ref=src, dst_ref=dst, send_sem=ts.at[kind, index], recv_sem=tr.at[kind, index],
            device_id={"tp": 1 - core}, device_id_type=MESH,
        )

    def span(q):
        return pl.ds(pl.multiple_of(q * LENGTH, LENGTH), LENGTH)

    def norm_copy(kind, q):
        return t_copy(2 * kind, q, ss.at[kind, span(q)], ssr.at[kind, span(q)])

    def mixer_copy(q):
        return t_copy(1, q, sent.at[:, span(q)], recv.at[:, span(q)])

    def cn_copy(q, side):
        return t_copy(3, q, cn.at[side, span(q)], cn.at[side, span(q)])

    def down_copy(index):
        return t_copy(4, index, sent.at[index], recv.at[index])

    def line(ref):
        return ref[...].astype(jnp.float32).reshape(1, -1)

    def sum_squares(kind, q):
        values = xm[span(q)].astype(jnp.float32)
        total = jnp.sum(values * values, axis=1, keepdims=True)
        ss[kind, span(q)] = jnp.broadcast_to(total, (LENGTH, ss.shape[2]))

    def inverse(kind, q):
        norm_copy(kind, q).wait_recv()
        total = ss[kind, span(q)][:, :1] + ssr[kind, span(q)][:, :1]
        return lax.rsqrt(total / width + EPS)

    def pool_piece(q):
        values = xm[span(q)].astype(jnp.float32)
        normed = (values * inverse(0, q) * line(mix_gain)).astype(jnp.bfloat16)
        at = lax.broadcasted_iota(jnp.int32, (LENGTH, LENGTH), 0)
        to = lax.broadcasted_iota(jnp.int32, (LENGTH, LENGTH), 1)
        for local in range(groups):
            reach = jnp.left_shift(jnp.int32(1), core * groups + local)
            lower = jnp.maximum(at - reach, 0)
            upper = jnp.minimum(at + reach, LENGTH)
            band = jnp.where((to >= lower) & (to < upper), 1.0, 0.0).astype(jnp.bfloat16)
            count = (upper[:, :1] - lower[:, :1]).astype(jnp.float32)
            part = normed[:, local * group : (local + 1) * group]
            pooled = dot(band, part) / count - part.astype(jnp.float32)
            cn[1 - core, span(q), local * group : (local + 1) * group] = pooled.astype(jnp.bfloat16)

    def mix_piece(q):
        grouped = []
        for local in range(groups):
            pooled = cn[1 - core, span(q), local * group : (local + 1) * group]
            linear = jnp.concatenate(
                [poolb[s * pool_rows + local * lane : s * pool_rows + (local + 1) * lane, :] for s in range(shards)], axis=0
            )
            product = lax.dot_general(pooled, linear, (((1,), (1,)), ((), ())), preferred_element_type=jnp.float32)
            grouped.append((product * pool_scale[local : local + 1, :]).astype(jnp.bfloat16))
        grouped = jnp.concatenate(grouped, axis=1)
        for target, side in ((sent, 1 - core), (keep, core)):

            def one(index, carry):
                start = pl.multiple_of((side * blocks + index) * half, TILE)
                target[index, span(q)] = dot(grouped, outb[pl.ds(start, half), :]).astype(jnp.bfloat16)
                return carry

            lax.fori_loop(0, blocks, one, 0)

    def both(q):
        return jnp.concatenate(
            [keep[i, span(q)].astype(jnp.float32) + recv[i, span(q)].astype(jnp.float32) for i in range(blocks)], axis=1
        )

    def middle_piece(q):
        copy = mixer_copy(q)
        copy.wait_recv()
        copy.wait_send()
        xm[span(q)] = (xm[span(q)].astype(jnp.float32) + both(q) * line(out_scale)).astype(jnp.bfloat16)
        sum_squares(1, q)

    def cn_piece(q):
        values = xm[span(q)].astype(jnp.float32)
        cn[core, span(q)] = (values * inverse(1, q) * line(channel_gain)).astype(jnp.bfloat16)

    def mixer_step(t):
        @pl.when(t >= 2)
        def _():
            cn_piece(t - 2)

        @pl.when((t >= 1) & (t <= seqs))
        def _():
            middle_piece(t - 1)
            norm_copy(1, t - 1).start()

        @pl.when(t < seqs)
        def _():
            mix_piece(t)
            mixer_copy(t).start()

        @pl.when(t >= 2)
        def _():
            cn_copy(t - 2, core).start()

    def wide(q, weight):
        return dot(cn[0, span(q)], weight[:half, :]) + dot(cn[1, span(q)], weight[half:, :])

    def lift_piece(q):
        cn_copy(q, 1 - core).wait_recv()
        lift[span(q)] = (wide(q, upb) * line(up_scale)).astype(jnp.bfloat16)

    def hidden_piece(q):
        gated = wide(q, gateb) * line(gate_scale)
        lifted = lift[span(q)].astype(jnp.float32)
        at = lax.broadcasted_iota(jnp.int32, (LENGTH, 1), 0)
        before = jnp.where(at == 0, 0.0, pltpu.roll(lifted, 1, 0))
        after = jnp.where(at == LENGTH - 1, 0.0, pltpu.roll(lifted, LENGTH - 1, 0))
        conv = (
            conv_weight[0:1, :] * before
            + conv_weight[1:2, :] * lifted
            + conv_weight[2:3, :] * after
        )
        lift[span(q)] = (jax.nn.gelu(conv) * gated).astype(jnp.bfloat16)

    loads = [
        pltpu.make_async_copy(out_in, s_out, in_sem.at[0]),
        pltpu.make_async_copy(pool_in, s_pool, in_sem.at[1]),
        pltpu.make_async_copy(x_in, xm, in_sem.at[2]),
        pltpu.make_async_copy(up_in, s_up, in_sem.at[3]),
        pltpu.make_async_copy(gate_in, s_gate, in_sem.at[4]),
        pltpu.make_async_copy(down_in, s_down, in_sem.at[5]),
    ] + [pltpu.make_async_copy(src, dst, in_sem.at[6 + i]) for i, (src, dst) in enumerate(zip(small_in, small))]
    for load in loads:
        load.start()
    barrier = pltpu.get_barrier_semaphore()
    for peer in ({"rep": 1 - r}, {"fs": 2 * a + 1 - b}, {"tp": 1 - core}):
        pl.semaphore_signal(barrier, inc=1, device_id=peer, device_id_type=MESH)

    @pl.when(a > 0)
    def _():
        pl.semaphore_signal(barrier, inc=1, device_id={"fs": f - 2}, device_id_type=MESH)

    @pl.when(a < n - 1)
    def _():
        pl.semaphore_signal(barrier, inc=1, device_id={"fs": f + 2}, device_id_type=MESH)

    def settle(load, staged, full):
        loads[load].wait()
        count = staged.shape[0]
        full[pl.ds(pl.multiple_of(f * count, TILE), count), :] = staged[...].astype(jnp.bfloat16)

    settle(1, s_pool, poolb)
    settle(0, s_out, outb)
    ends = jnp.where(a > 0, 1, 0) + jnp.where(a < n - 1, 1, 0)
    pl.semaphore_wait(barrier, 3 + ends)

    pool_c, out_c, up_c, gate_c = chunks[:4]
    down_c = chunks[4:]
    begin(pool_c)
    begin(out_c)
    settle(3, s_up, upb)
    for load in loads[2:3] + loads[6:]:
        load.wait()

    def first_sum(q, carry):
        sum_squares(0, q)
        return carry

    lax.fori_loop(0, seqs, first_sum, 0)
    begin(up_c)

    def first_send(q, carry):
        norm_copy(0, q).start()
        return carry

    lax.fori_loop(0, seqs, first_send, 0)
    settle(4, s_gate, gateb)
    settle(5, s_down, downb)

    stage([pool_c, out_c], lambda: None, pool_piece, seqs)
    begin(gate_c)
    stage([up_c], lambda: arrived([pool_c, out_c]), mixer_step, seqs + 2)
    for chunk in down_c:
        begin(chunk)
    stage([gate_c], lambda: arrived([up_c]), lift_piece, seqs)
    stage(down_c, lambda: arrived([gate_c]), hidden_piece, seqs)

    shard_rows = s_down.shape[0]

    def down_step(i, carry):
        j, kind = i // 2, i % 2
        s = order(j)

        @pl.when(kind == 1)
        def _():
            for chunk in down_c:
                x_wait(chunk, j, 1)

        @pl.when((kind == 0) & (j > 0))
        def _():
            for chunk in down_c:
                x_wait(chunk, j, 0)

        shard = 2 * s + (b + kind) % 2
        start = pl.multiple_of(shard * shard_rows, TILE)
        side, index = shard // blocks, shard % blocks
        product = dot(lift[...], downb[pl.ds(start, shard_rows), :]).astype(jnp.bfloat16)

        @pl.when(side == core)
        def _():
            keep[index] = product

        @pl.when(side != core)
        def _():
            sent[index] = product
            down_copy(index).start()

        return carry

    lax.fori_loop(0, shards, down_step, 0)

    def down_wait(index, carry):
        down_copy(index).wait_recv()
        return carry

    lax.fori_loop(0, blocks, down_wait, 0)

    def last(q, carry):
        o_ref[span(q), :] = (xm[span(q)].astype(jnp.float32) + both(q) * line(down_scale)).astype(jnp.bfloat16)
        return carry

    lax.fori_loop(0, seqs, last, 0)

    for chunk in chunks:
        finish(chunk)

    def sends(q, carry):
        norm_copy(0, q).wait_send()
        norm_copy(1, q).wait_send()
        cn_copy(q, core).wait_send()
        return carry

    lax.fori_loop(0, seqs, sends, 0)

    def down_sends(index, carry):
        down_copy(index).wait_send()
        return carry

    lax.fori_loop(0, blocks, down_sends, 0)


def per_device(
    shards,
    layer_in,
    mix_gain,
    pool_weight,
    pool_scale,
    out_weight,
    out_scale,
    channel_gain,
    up_weight,
    up_scale,
    gate_weight,
    gate_scale,
    conv_weight,
    down_weight,
    down_scale,
):
    rows, half = layer_in.shape
    n = shards // 2
    hidden_width = up_weight.shape[1]
    groups, group, lane = pool_weight.shape
    block = out_weight.shape[1]
    blocks = half // block
    seqs = rows // LENGTH
    pool_rows = jnp.transpose(pool_weight, (0, 2, 1)).reshape(groups * lane, group)
    small = (
        mix_gain,
        pool_scale,
        out_scale.reshape(1, -1),
        channel_gain,
        up_scale,
        gate_scale,
        conv_weight,
        down_scale.reshape(1, -1),
    )
    heights = (groups * lane, half, up_weight.shape[0], gate_weight.shape[0])
    chunks = [Chunk(i, i, h, 0, h, ALONG[i], ACROSS[i]) for i, h in enumerate(heights)]
    cut = hidden_width // 2 // TILE * TILE
    for offset, height in ((0, cut), (cut, hidden_width - cut)):
        chunks.append(Chunk(len(chunks), 4, hidden_width, offset, height, ALONG[4], ACROSS[4]))
    count = len(chunks)
    bf16, f32 = jnp.bfloat16, jnp.float32
    dma = pltpu.SemaphoreType.DMA
    return pl.pallas_call(
        functools.partial(layer_kernel, n, chunks),
        out_shape=jax.ShapeDtypeStruct((rows, half), bf16),
        in_specs=[pl.BlockSpec(memory_space=pl.ANY)] * (6 + len(small)),
        out_specs=pl.BlockSpec(memory_space=pltpu.VMEM),
        scratch_shapes=[pltpu.VMEM(v.shape, v.dtype) for v in small]
        + [
            pltpu.VMEM((shards * groups * lane, group), bf16),
            pltpu.VMEM((shards * half, block), bf16),
            pltpu.VMEM((shards * up_weight.shape[0], hidden_width), bf16),
            pltpu.VMEM((shards * gate_weight.shape[0], hidden_width), bf16),
            pltpu.VMEM((shards * hidden_width, block), bf16),
            pltpu.VMEM(pool_rows.shape, f32),
            pltpu.VMEM(out_weight.shape, f32),
            pltpu.VMEM(up_weight.shape, f32),
            pltpu.VMEM(gate_weight.shape, f32),
            pltpu.VMEM(down_weight.shape, f32),
            pltpu.VMEM((rows, half), bf16),
            pltpu.VMEM((blocks, rows, block), bf16),
            pltpu.VMEM((blocks, rows, block), bf16),
            pltpu.VMEM((blocks, rows, block), bf16),
            pltpu.VMEM((2, rows, half), bf16),
            pltpu.VMEM((rows, hidden_width), bf16),
            pltpu.VMEM((2, rows, 128), f32),
            pltpu.VMEM((2, rows, 128), f32),
            dma((6 + len(small),)),
            dma((count, n + 1)),
            dma((count, n)),
            dma((count, n)),
            dma((count, n)),
            dma((count, 2, n)),
            dma((count, 2, n)),
            dma((5, max(seqs, blocks))),
            dma((5, max(seqs, blocks))),
        ],
        compiler_params=pltpu.CompilerParams(
            collective_id=0, has_side_effects=True, vmem_limit_bytes=67_043_328
        ),
        name="layer",
    )(layer_in, pool_rows, out_weight, up_weight, gate_weight, down_weight, *small)


def solution(mesh):
    placed = (
        P(("rep", "fs"), "tp"),
        P("tp"),
        P("tp", None, "fs"),
        P("tp", None),
        P("tp", "fs"),
        P("tp"),
        P("tp"),
        P("fs", "tp"),
        P("tp"),
        P("fs", "tp"),
        P("tp"),
        P(None, "tp"),
        P("tp", "fs"),
        P("tp"),
    )
    body = functools.partial(per_device, mesh.shape["fs"])
    return jax.shard_map(
        body, mesh=mesh, in_specs=placed, out_specs=P(("rep", "fs"), "tp"), check_vma=False
    )
```

profile of v0, /device:TPU:1, one launch (start us, length us, event | category | flops | bytes accessed | tf_op | source)
XLA Modules:
  0.0 195.7 jit_solution(1861655770044790843)
XLA Ops:
  0.0 192.6 %layer.1 = bf16[1024,1024]{1,0:T(8,128)(2,1)} custom-call(bf16[1024,1024]{1,0:T(8,128)(2,1)} %refs_0_.1, f32[128,512]{1,0:T(8,128)} %bitcast.5, f32[1024,256]{1,0:T(8,128)} %refs_2_.1, f32[256,1408]{1,0:T(8,128)} %refs_3_.1, f32[256,1408]{1,0:T(8,128)} %refs_4_.1, f32[1408,256]{1,0:T(8,128)} %refs_5_.1, bf16[1024]{0:T(1024)(128)(2,1)} %refs_6_.1, ...), custom_call_target="tpu_custom_call" | custom-call | tf_op jit(solution)/shard_map/layer/pallas_call | solution.py:488
  192.6 3.1 %copy.16 = bf16[1024,1024]{1,0:T(8,128)(2,1)} copy(bf16[1024,1024]{1,0:T(8,128)(2,1)} %layer.1) | data formatting | bytes 4194304
where the time goes:
time: 196 us
  Pallas kernels  193 us (98%)
  local copies, waits for them, and re-layouts  3.08 us (2%)
    pallas_call x1, Pallas kernels, per_device(): pl.pallas_call(functools.partial(layer_kernel, n, chunks), out_shape=jax....  193 us

commit v1 on v0

--- a/solution.py
+++ b/solution.py
@@ -12,29 +12,108 @@
 TILE = 16
 MESH = pl.DeviceIdType.MESH
 
-ALONG = (0.78, 0.78, 0.78, 0.78, 0.72)
-ACROSS = (0.58, 0.58, 0.58, 0.58, 0.60)
+PLAN = (
+    (0, 0, 1, 0.75, 0.5, 0.5),
+    (1, 0, 2, 0.6562, 0.5312, 0.5938),
+    (1, 1, 2, 0.7188, 0.5, 0.5),
+    (2, 0, 2, 0.625, 0.5, 0.625),
+    (2, 1, 2, 0.75, 0.5, 0.625),
+    (3, 0, 2, 0.75, 0.5, 0.75),
+    (3, 1, 2, 0.75, 0.5, 0.625),
+    (4, 0, 4, 0.9091, 0.5455, 0.5),
+    (4, 1, 4, 0.9091, 0.5909, 0.6818),
+    (4, 2, 4, 0.7727, 0.6364, 0.7273),
+    (4, 3, 4, 0.8636, 0.5909, 0.5909),
+)
+HEAD = 2
+SEND, ALONG, ACROSS, ARRIVED = "send", "along", "across", "arrived"
+
+ENDS = (
+    ((ACROSS, 0, 0),),
+    ((ALONG, 0, 1), (SEND, 2, 0),),
+    ((ACROSS, 1, 0),),
+    (),
+    ((ALONG, 1, 1), (SEND, 3, 0), (ACROSS, 0, 1), (ACROSS, 2, 0), (ALONG, 0, 2), (ALONG, 2, 1), (SEND, 4, 0), (ACROSS, 1, 1), (ACROSS, 3, 0), (ALONG, 1, 2), (ALONG, 3, 1), (SEND, 5, 0), (ACROSS, 2, 1), (ACROSS, 0, 2), (ACROSS, 4, 0), (ALONG, 2, 2), (ALONG, 0, 3), (ACROSS, 3, 1), (ALONG, 4, 1), (SEND, 6, 0), (ACROSS, 1, 2), (ACROSS, 5, 0), (ACROSS, 2, 2), (ALONG, 1, 3), (ALONG, 3, 2), (ALONG, 5, 1), (SEND, 7, 0), (ACROSS, 0, 3), (ACROSS, 4, 1), (ACROSS, 6, 0), (ALONG, 2, 3), (ALONG, 6, 1), (SEND, 8, 0), (ACROSS, 1, 3), (ACROSS, 5, 1), (ACROSS, 3, 2), (ACROSS, 7, 0), (ALONG, 4, 2), (ALONG, 7, 1), (SEND, 9, 0), (ALONG, 3, 3), (ACROSS, 2, 3), (ACROSS, 6, 1), (ACROSS, 8, 0), (ALONG, 5, 2), (ACROSS, 4, 2), (ALONG, 8, 1), (SEND, 10, 0), (ACROSS, 7, 1), (ALONG, 4, 3), (ACROSS, 3, 3), (ACROSS, 9, 0), (ARRIVED, 1, 0),),
+    ((ALONG, 9, 1), (ALONG, 6, 2), (ACROSS, 5, 2),),
+    ((ALONG, 5, 3),),
+    ((ACROSS, 8, 1),),
+    ((ACROSS, 10, 0),),
+    ((ACROSS, 4, 3),),
+    ((ALONG, 7, 2), (ALONG, 6, 3), (ALONG, 10, 1), (ACROSS, 9, 1), (ACROSS, 6, 2), (ACROSS, 5, 3), (ALONG, 8, 2), (ARRIVED, 2, 0),),
+    ((ALONG, 7, 3), (ACROSS, 7, 2),),
+    ((ALONG, 9, 2),),
+    ((ACROSS, 6, 3), (ACROSS, 10, 1),),
+    ((ALONG, 8, 3), (ACROSS, 8, 2), (ALONG, 10, 2), (ACROSS, 7, 3), (ALONG, 9, 3), (ARRIVED, 3, 0),),
+    ((ACROSS, 9, 2), (ALONG, 10, 3),),
+    ((ACROSS, 8, 3),),
+    ((ACROSS, 10, 2),),
+    ((ACROSS, 9, 3), (ACROSS, 10, 3),),
+)
+MIDDLES = (
+    ((ACROSS, 0, 0),),
+    ((ALONG, 0, 1), (SEND, 2, 0), (ALONG, 0, 2),),
+    ((ACROSS, 1, 0),),
+    (),
+    ((ALONG, 1, 1), (SEND, 3, 0), (ALONG, 1, 2), (ACROSS, 0, 1), (ACROSS, 2, 0), (ALONG, 2, 2), (ALONG, 0, 3), (ACROSS, 0, 2), (ALONG, 2, 1), (SEND, 4, 0), (ACROSS, 1, 1), (ALONG, 3, 2), (ACROSS, 3, 0), (ALONG, 3, 1), (SEND, 5, 0), (ALONG, 1, 3), (ACROSS, 1, 2), (ACROSS, 2, 2), (ALONG, 2, 3), (ALONG, 4, 1), (SEND, 6, 0), (ALONG, 4, 2), (ACROSS, 0, 3), (ACROSS, 2, 1), (ACROSS, 4, 0), (ALONG, 5, 1), (SEND, 7, 0), (ALONG, 5, 2), (ALONG, 3, 3), (ACROSS, 3, 1), (ACROSS, 3, 2), (ACROSS, 1, 3), (ACROSS, 5, 0), (ALONG, 6, 1), (SEND, 8, 0), (ALONG, 4, 3), (ALONG, 6, 2), (ALONG, 7, 1), (SEND, 9, 0), (ALONG, 5, 3), (ACROSS, 2, 3), (ACROSS, 4, 1), (ALONG, 7, 2), (ACROSS, 4, 2), (ACROSS, 6, 0), (ALONG, 8, 1), (SEND, 10, 0), (ALONG, 6, 3), (ALONG, 8, 2), (ALONG, 9, 1), (ALONG, 7, 3), (ACROSS, 5, 1), (ACROSS, 5, 2), (ACROSS, 3, 3), (ACROSS, 7, 0), (ALONG, 9, 2), (ALONG, 8, 3), (ALONG, 10, 1), (ALONG, 9, 3), (ACROSS, 6, 1), (ALONG, 10, 2), (ARRIVED, 1, 0),),
+    ((ACROSS, 8, 0),),
+    ((ACROSS, 6, 2), (ACROSS, 4, 3),),
+    ((ALONG, 10, 3),),
+    (),
+    ((ACROSS, 7, 1),),
+    ((ACROSS, 9, 0), (ACROSS, 5, 3), (ACROSS, 7, 2), (ACROSS, 8, 1), (ACROSS, 6, 3), (ACROSS, 10, 0), (ARRIVED, 2, 0),),
+    (),
+    ((ACROSS, 8, 2),),
+    ((ACROSS, 9, 1),),
+    ((ACROSS, 7, 3), (ARRIVED, 3, 0),),
+    ((ACROSS, 9, 2), (ACROSS, 8, 3),),
+    ((ACROSS, 10, 1),),
+    (),
+    ((ACROSS, 9, 3), (ACROSS, 10, 2), (ACROSS, 10, 3),),
+)
 
 
 class Chunk:
-    def __init__(self, index, buffer, shard, offset, rows, along, across):
-        units = rows // TILE
-        least = (units + 1) // 2
-        self.index, self.buffer, self.shard, self.offset, self.rows = index, buffer, shard, offset, rows
-        self.along = TILE * min(max(round(units * along), least), units)
-        self.across = min(TILE * max(round(units * across), least), self.along)
+    def __init__(self, index, weight, shard, part, parts, along, across_own, across):
+        units = shard // TILE
+        first, last = units * part // parts, units * (part + 1) // parts
+        count = last - first
+        least = (count + 1) // 2
+        self.index, self.weight, self.shard = index, weight, shard
+        self.offset, self.rows = first * TILE, count * TILE
+
+        def share(fraction, most):
+            return TILE * min(max(round(count * fraction), least), most)
+
+        self.along = share(along, count)
+        self.across_own = share(across_own, count)
+        self.across = share(across, self.along // TILE)
+
+
+def plain(chunks, n, seqs):
+    counts = {0: seqs, 1: seqs + 2, 2: seqs, 3: seqs}
+    segments = [[(SEND, chunk.index, 0) for chunk in chunks[HEAD:]]] + [[] for _ in range(seqs)]
+    for weight in range(5):
+        for chunk in chunks:
+            if chunk.weight == weight:
+                for j in range(1, n):
+                    segments[-1] += [(ALONG, chunk.index, j), (ACROSS, chunk.index, j - 1)]
+                segments[-1].append((ACROSS, chunk.index, n - 1))
+        if 1 <= weight <= 3:
+            segments[-1].append((ARRIVED, weight, 0))
+            segments += [[] for _ in range(counts[weight])]
+    return segments
 
 
 def dot(left, right):
     return jnp.dot(left, right, preferred_element_type=jnp.float32)
 
 
-def layer_kernel(n, chunks, *refs):
+def layer_kernel(n, chunks, segments, *refs):
     x_in, pool_in, out_in, up_in, gate_in, down_in = refs[:6]
     small_in, o_ref, small = refs[6:14], refs[14], refs[15:23]
     poolb, outb, upb, gateb, downb, s_pool, s_out, s_up, s_gate, s_down = refs[23:33]
     xm, keep, sent, recv, cn, lift, ss, ssr = refs[33:41]
-    in_sem, zs, zr, ys, yr, xs, xr, ts, tr = refs[41:]
+    in_sem, out_sem, zs, zr, ys, yr, xs, xr, ts, tr = refs[41:]
     mix_gain, pool_scale, out_scale, channel_gain, up_scale, gate_scale, conv_weight, down_scale = small
     buffers = (poolb, outb, upb, gateb, downb)
 
@@ -61,7 +140,7 @@
 
     def rows_of(chunk, shard, start, count):
         begin = pl.multiple_of(shard * chunk.shard + chunk.offset + start, TILE)
-        return buffers[chunk.buffer].at[pl.ds(begin, count)]
+        return buffers[chunk.weight].at[pl.ds(begin, count)]
 
     def z_copy(chunk, s, target, slot):
         part = rows_of(chunk, 2 * s + b, r * (chunk.rows - chunk.along), chunk.along)
@@ -70,15 +149,16 @@
             device_id={"fs": 2 * target + b}, device_id_type=MESH,
         )
 
-    def y_copy(chunk, s, side):
-        part = rows_of(chunk, 2 * s + side, r * (chunk.rows - chunk.across), chunk.across)
+    def y_copy(chunk, s, side, own):
+        had = chunk.across_own if own else chunk.across
+        part = rows_of(chunk, 2 * s + side, r * (chunk.rows - had), had)
         return pltpu.make_async_remote_copy(
             src_ref=part, dst_ref=part, send_sem=ys.at[chunk.index, s], recv_sem=yr.at[chunk.index, s],
             device_id={"fs": 2 * a + 1 - b}, device_id_type=MESH,
         )
 
-    def x_copy(chunk, s, kind, end):
-        had = chunk.across if kind else chunk.along
+    def x_copy(chunk, s, kind, end, own=False):
+        had = chunk.along if kind == 0 else chunk.across_own if own else chunk.across
         part = rows_of(chunk, 2 * s + (1 - b if kind else b), end * had, chunk.rows - had)
         return pltpu.make_async_remote_copy(
             src_ref=part, dst_ref=part, send_sem=xs.at[chunk.index, kind, s], recv_sem=xr.at[chunk.index, kind, s],
@@ -98,7 +178,7 @@
         def _():
             z_copy(chunk, a, a - 1, n).start()
 
-        y_copy(chunk, a, b).start()
+        y_copy(chunk, a, b, True).start()
 
     def z_event(chunk, j):
         s = order(j)
@@ -109,32 +189,33 @@
         def _():
             z_copy(chunk, s, target, s).start()
 
-        y_copy(chunk, s, b).start()
+        y_copy(chunk, s, b, False).start()
         if chunk.rows > chunk.along:
             x_copy(chunk, s, 0, r).start()
 
     def y_event(chunk, j):
         s = order(j)
-        y_copy(chunk, s, 1 - b).wait_recv()
-        if chunk.rows > chunk.across:
-            x_copy(chunk, s, 1, r).start()
-
-    def x_wait(chunk, j, kind):
-        if kind and chunk.rows > chunk.across:
-            x_copy(chunk, order(j), 1, 1 - r).wait_recv()
-        if not kind and chunk.rows > chunk.along:
-            x_copy(chunk, order(j), 0, 1 - r).wait_recv()
-
-    def arrived(which):
-        for chunk in which:
-            x_wait(chunk, 0, 1)
-
-            def step(j, carry):
-                x_wait(chunk, j, 0)
-                x_wait(chunk, j, 1)
-                return carry
-
-            lax.fori_loop(1, n, step, 0)
+        own = j == 0
+        y_copy(chunk, s, 1 - b, own).wait_recv()
+        if chunk.rows > (chunk.across_own if own else chunk.across):
+            x_copy(chunk, s, 1, r, own).start()
+
+    def x_wait(chunk, j, kind, own=False):
+        had = chunk.along if kind == 0 else chunk.across_own if own else chunk.across
+        if chunk.rows > had:
+            x_copy(chunk, order(j), kind, 1 - r, own).wait_recv()
+
+    def arrived(weights):
+        for chunk in chunks:
+            if chunk.weight in weights:
+                x_wait(chunk, 0, 1, True)
+
+                def step(j, carry):
+                    x_wait(chunk, j, 0)
+                    x_wait(chunk, j, 1)
+                    return carry
+
+                lax.fori_loop(1, n, step, 0)
 
     def finish(chunk):
         @pl.when(a < n - 1)
@@ -144,53 +225,67 @@
         @pl.when(a > 0)
         def _():
             z_copy(chunk, a, a - 1, n).wait_send()
+
+        y_copy(chunk, a, b, True).wait_send()
+        if chunk.rows > chunk.across_own:
+            x_copy(chunk, a, 1, r, True).wait_send()
 
         def step(j, carry):
             s = order(j)
             target, valid = onward(s)
-            y_copy(chunk, s, b).wait_send()
+            y_copy(chunk, s, b, False).wait_send()
             if chunk.rows > chunk.across:
                 x_copy(chunk, s, 1, r).wait_send()
-
-            @pl.when(j > 0)
+            if chunk.rows > chunk.along:
+                x_copy(chunk, s, 0, r).wait_send()
+
+            @pl.when(valid)
             def _():
-                if chunk.rows > chunk.along:
-                    x_copy(chunk, s, 0, r).wait_send()
-
-                @pl.when(valid)
-                def _():
-                    z_copy(chunk, s, target, s).wait_send()
+                z_copy(chunk, s, target, s).wait_send()
 
             return carry
 
-        lax.fori_loop(0, n, step, 0)
-
-    def stage(which, before, piece, count):
-        for chunk in which:
-            z_event(chunk, 1)
-        for chunk in which:
-            y_event(chunk, 0)
-        before()
-
-        def step(j, carry):
-            def one(q, inner):
-                piece(q)
-                return inner
-
-            lax.fori_loop((j - 1) * count // (n - 1), j * count // (n - 1), one, 0)
-
-            @pl.when(j < n - 1)
-            def _():
-                for chunk in which:
-                    z_event(chunk, j + 1)
-                for chunk in which:
-                    y_event(chunk, j)
+        lax.fori_loop(1, n, step, 0)
+
+    def events(segment):
+        for name, index, j in segment:
+            if name == SEND:
+                begin(chunks[index])
+            elif name == ALONG:
+                z_event(chunks[index], j)
+            elif name == ACROSS:
+                y_event(chunks[index], j)
+            else:
+                arrived((0, 1) if index == 1 else (index,))
+
+    inner = (a > 0) & (a < n - 1)
+
+    def between(ends, middles):
+        if ends == middles:
+            events(ends)
+            return
+
+        @pl.when(jnp.logical_not(inner))
+        def _():
+            events(ends)
+
+        @pl.when(inner)
+        def _():
+            events(middles)
+
+    def stage(first, count, piece):
+        def step(q, carry):
+            piece(q)
+            for i in range(count):
+                if segments[0][first + i] or segments[1][first + i]:
+
+                    @pl.when(q == i)
+                    def _(i=i):
+                        between(segments[0][first + i], segments[1][first + i])
 
             return carry
 
-        lax.fori_loop(1, n, step, 0)
-        for chunk in which:
-            y_event(chunk, n - 1)
+        lax.fori_loop(0, count, step, 0)
 
     def t_copy(kind, index, src, dst):
         return pltpu.make_async_remote_copy(
@@ -347,10 +442,8 @@
     ends = jnp.where(a > 0, 1, 0) + jnp.where(a < n - 1, 1, 0)
     pl.semaphore_wait(barrier, 3 + ends)
 
-    pool_c, out_c, up_c, gate_c = chunks[:4]
-    down_c = chunks[4:]
-    begin(pool_c)
-    begin(out_c)
+    for chunk in chunks[:HEAD]:
+        begin(chunk)
     settle(3, s_up, upb)
     for load in loads[2:3] + loads[6:]:
         load.wait()
@@ -360,7 +453,6 @@
         return carry
 
     lax.fori_loop(0, seqs, first_sum, 0)
-    begin(up_c)
 
     def first_send(q, carry):
         norm_copy(0, q).start()
@@ -369,14 +461,16 @@
     lax.fori_loop(0, seqs, first_send, 0)
     settle(4, s_gate, gateb)
     settle(5, s_down, downb)
-
-    stage([pool_c, out_c], lambda: None, pool_piece, seqs)
-    begin(gate_c)
-    stage([up_c], lambda: arrived([pool_c, out_c]), mixer_step, seqs + 2)
-    for chunk in down_c:
-        begin(chunk)
-    stage([gate_c], lambda: arrived([up_c]), lift_piece, seqs)
-    stage(down_c, lambda: arrived([gate_c]), hidden_piece, seqs)
+    between(segments[0][0], segments[1][0])
+
+    stage(1, seqs, pool_piece)
+    stage(1 + seqs, seqs + 2, mixer_step)
+    stage(3 + 2 * seqs, seqs, lift_piece)
+    stage(3 + 3 * seqs, seqs, hidden_piece)
+    down_c = [chunk for chunk in chunks if chunk.weight == 4]
+    for chunk in chunks:
+        if chunk.weight < 3:
+            finish(chunk)
 
     shard_rows = s_down.shape[0]
 
@@ -384,7 +478,12 @@
         j, kind = i // 2, i % 2
         s = order(j)
 
-        @pl.when(kind == 1)
+        @pl.when((kind == 1) & (j == 0))
+        def _():
+            for chunk in down_c:
+                x_wait(chunk, 0, 1, True)
+
+        @pl.when((kind == 1) & (j > 0))
         def _():
             for chunk in down_c:
                 x_wait(chunk, j, 1)
@@ -418,19 +517,25 @@
 
     lax.fori_loop(0, blocks, down_wait, 0)
 
+    def result(q):
+        return pltpu.make_async_copy(xm.at[span(q)], o_ref.at[span(q)], out_sem.at[q])
+
     def last(q, carry):
-        o_ref[span(q), :] = (xm[span(q)].astype(jnp.float32) + both(q) * line(down_scale)).astype(jnp.bfloat16)
+        xm[span(q)] = (xm[span(q)].astype(jnp.float32) + both(q) * line(down_scale)).astype(jnp.bfloat16)
+        result(q).start()
         return carry
 
     lax.fori_loop(0, seqs, last, 0)
 
     for chunk in chunks:
-        finish(chunk)
+        if chunk.weight >= 3:
+            finish(chunk)
 
     def sends(q, carry):
         norm_copy(0, q).wait_send()
         norm_copy(1, q).wait_send()
         cn_copy(q, core).wait_send()
+        result(q).wait()
         return carry
 
     lax.fori_loop(0, seqs, sends, 0)
@@ -477,19 +582,17 @@
         conv_weight,
         down_scale.reshape(1, -1),
     )
-    heights = (groups * lane, half, up_weight.shape[0], gate_weight.shape[0])
-    chunks = [Chunk(i, i, h, 0, h, ALONG[i], ACROSS[i]) for i, h in enumerate(heights)]
-    cut = hidden_width // 2 // TILE * TILE
-    for offset, height in ((0, cut), (cut, hidden_width - cut)):
-        chunks.append(Chunk(len(chunks), 4, hidden_width, offset, height, ALONG[4], ACROSS[4]))
+    heights = (groups * lane, half, up_weight.shape[0], gate_weight.shape[0], hidden_width)
+    chunks = [Chunk(i, entry[0], heights[entry[0]], *entry[1:]) for i, entry in enumerate(PLAN)]
+    segments = (ENDS, MIDDLES) if n == 4 and seqs == 4 else (plain(chunks, n, seqs),) * 2
     count = len(chunks)
     bf16, f32 = jnp.bfloat16, jnp.float32
     dma = pltpu.SemaphoreType.DMA
     return pl.pallas_call(
-        functools.partial(layer_kernel, n, chunks),
+        functools.partial(layer_kernel, n, chunks, segments),
         out_shape=jax.ShapeDtypeStruct((rows, half), bf16),
         in_specs=[pl.BlockSpec(memory_space=pl.ANY)] * (6 + len(small)),
-        out_specs=pl.BlockSpec(memory_space=pltpu.VMEM),
+        out_specs=pl.BlockSpec(memory_space=pl.ANY),
         scratch_shapes=[pltpu.VMEM(v.shape, v.dtype) for v in small]
         + [
             pltpu.VMEM((shards * groups * lane, group), bf16),
@@ -511,6 +614,7 @@
             pltpu.VMEM((2, rows, 128), f32),
             pltpu.VMEM((2, rows, 128), f32),
             dma((6 + len(small),)),
+            dma((seqs,)),
             dma((count, n + 1)),
             dma((count, n)),
             dma((count, n)),

time: 196 us -> 168 us (0.86)
  Pallas kernels: 193 us -> 165 us
    pallas_call x1, Pallas kernels: 193 us -> 165 us  [per_device(): pl.pallas_call(functools.partial(layer_kernel, n, chunks, segments), out_...]
where the time goes in v1:
time: 168 us
  Pallas kernels  165 us (98%)
  local copies, waits for them, and re-layouts  3.08 us (2%)
    pallas_call x1, Pallas kernels, per_device(): pl.pallas_call(functools.partial(layer_kernel, n, chunks, segments), out_...  165 us

profile of v1, /device:TPU:1, one launch (start us, length us, event | category | flops | bytes accessed | tf_op | source)
XLA Modules:
  0.0 168.2 jit_solution(12370037681627760758)
XLA Ops:
  0.0 165.1 %layer.1 = bf16[1024,1024]{1,0:T(8,128)(2,1)} custom-call(bf16[1024,1024]{1,0:T(8,128)(2,1)} %refs_0_.1, f32[128,512]{1,0:T(8,128)} %bitcast.5, f32[1024,256]{1,0:T(8,128)} %refs_2_.1, f32[256,1408]{1,0:T(8,128)} %refs_3_.1, f32[256,1408]{1,0:T(8,128)} %refs_4_.1, f32[1408,256]{1,0:T(8,128)} %refs_5_.1, bf16[1024]{0:T(1024)(128)(2,1)} %refs_6_.1, ...), custom_call_target="tpu_custom_call" | custom-call | tf_op jit(solution)/shard_map/layer/pallas_call | solution.py:591
  165.1 3.1 %copy.16 = bf16[1024,1024]{1,0:T(8,128)(2,1)} copy(bf16[1024,1024]{1,0:T(8,128)(2,1)} %layer.1) | data formatting | bytes 4194304

commit v2 on v1

--- a/solution.py
+++ b/solution.py
@@ -13,62 +13,78 @@
 MESH = pl.DeviceIdType.MESH
 
 PLAN = (
-    (0, 0, 1, 0.75, 0.5, 0.5),
-    (1, 0, 2, 0.6562, 0.5312, 0.5938),
-    (1, 1, 2, 0.7188, 0.5, 0.5),
-    (2, 0, 2, 0.625, 0.5, 0.625),
-    (2, 1, 2, 0.75, 0.5, 0.625),
-    (3, 0, 2, 0.75, 0.5, 0.75),
-    (3, 1, 2, 0.75, 0.5, 0.625),
-    (4, 0, 4, 0.9091, 0.5455, 0.5),
-    (4, 1, 4, 0.9091, 0.5909, 0.6818),
-    (4, 2, 4, 0.7727, 0.6364, 0.7273),
-    (4, 3, 4, 0.8636, 0.5909, 0.5909),
+    (0, 0, 1, 4, 5, 4),
+    (1, 0, 2, 16, 17, 16),
+    (1, 1, 2, 17, 16, 16),
+    (2, 0, 2, 4, 4, 4),
+    (2, 1, 2, 6, 4, 4),
+    (3, 0, 2, 8, 8, 5),
+    (3, 1, 2, 7, 4, 6),
+    (4, 0, 4, 20, 11, 17),
+    (4, 1, 4, 19, 11, 14),
+    (4, 2, 4, 20, 19, 11),
+    (4, 3, 4, 22, 17, 12),
 )
+UNITS = (8, 32, 32, 8, 8, 8, 8, 22, 22, 22, 22)
 HEAD = 2
-SEND, ALONG, ACROSS, ARRIVED = "send", "along", "across", "arrived"
+SEND_ALONG, SEND_ACROSS, ALONG, ACROSS, ARRIVED = range(5)
 
 ENDS = (
-    ((ACROSS, 0, 0),),
-    ((ALONG, 0, 1), (SEND, 2, 0),),
-    ((ACROSS, 1, 0),),
+    ((SEND_ACROSS, 4, 0), (SEND_ALONG, 2, 0), (SEND_ALONG, 3, 0), (ALONG, 0, 1), (SEND_ALONG, 9, 0), (ALONG, 1, 1),
+     (ALONG, 0, 2), (ACROSS, 1, 0),),
+    ((ALONG, 2, 1), (SEND_ALONG, 6, 0), (ALONG, 1, 2), (SEND_ACROSS, 3, 0), (SEND_ACROSS, 2, 0), (ACROSS, 4, 0),
+     (ACROSS, 1, 1), (SEND_ACROSS, 9, 0), (ACROSS, 1, 2), (ALONG, 1, 3), (SEND_ALONG, 4, 0), (ALONG, 4, 1),
+     (SEND_ALONG, 10, 0), (ALONG, 2, 3), (SEND_ACROSS, 8, 0), (ACROSS, 2, 1), (ACROSS, 1, 3), (ALONG, 2, 2),
+     (SEND_ACROSS, 6, 0), (ACROSS, 0, 1),),
+    ((ACROSS, 2, 0), (ACROSS, 0, 0), (ALONG, 7, 1), (ACROSS, 3, 0), (ACROSS, 2, 3), (ALONG, 0, 3), (ALONG, 3, 3),
+     (SEND_ACROSS, 10, 0),),
+    ((SEND_ACROSS, 5, 0), (ALONG, 3, 1), (ALONG, 6, 1), (ACROSS, 2, 2), (SEND_ALONG, 8, 0), (ACROSS, 0, 2),
+     (ACROSS, 10, 0), (ACROSS, 0, 3), (ACROSS, 5, 0), (ACROSS, 6, 0), (ACROSS, 8, 0),),
+    ((SEND_ALONG, 5, 0), (ALONG, 9, 3), (SEND_ACROSS, 7, 0), (ALONG, 5, 1), (ACROSS, 4, 1), (ACROSS, 6, 1),
+     (ALONG, 4, 2), (ARRIVED, 1, 0), (SEND_ALONG, 7, 0),),
+    ((ACROSS, 3, 3), (ALONG, 4, 3), (ALONG, 3, 2),),
+    ((ACROSS, 5, 1), (ALONG, 6, 3), (ACROSS, 4, 3), (ACROSS, 7, 1),),
+    ((ACROSS, 3, 1), (ALONG, 6, 2), (ALONG, 9, 2), (ACROSS, 3, 2), (ALONG, 5, 2),),
+    ((ACROSS, 4, 2), (ACROSS, 6, 2), (ACROSS, 9, 3), (ACROSS, 6, 3), (ALONG, 5, 3), (ALONG, 8, 1),),
+    ((ACROSS, 9, 0),),
+    ((ARRIVED, 2, 0), (ACROSS, 5, 3), (ACROSS, 5, 2), (ALONG, 9, 1), (ALONG, 8, 2), (ALONG, 10, 1),),
     (),
-    ((ALONG, 1, 1), (SEND, 3, 0), (ACROSS, 0, 1), (ACROSS, 2, 0), (ALONG, 0, 2), (ALONG, 2, 1), (SEND, 4, 0), (ACROSS, 1, 1), (ACROSS, 3, 0), (ALONG, 1, 2), (ALONG, 3, 1), (SEND, 5, 0), (ACROSS, 2, 1), (ACROSS, 0, 2), (ACROSS, 4, 0), (ALONG, 2, 2), (ALONG, 0, 3), (ACROSS, 3, 1), (ALONG, 4, 1), (SEND, 6, 0), (ACROSS, 1, 2), (ACROSS, 5, 0), (ACROSS, 2, 2), (ALONG, 1, 3), (ALONG, 3, 2), (ALONG, 5, 1), (SEND, 7, 0), (ACROSS, 0, 3), (ACROSS, 4, 1), (ACROSS, 6, 0), (ALONG, 2, 3), (ALONG, 6, 1), (SEND, 8, 0), (ACROSS, 1, 3), (ACROSS, 5, 1), (ACROSS, 3, 2), (ACROSS, 7, 0), (ALONG, 4, 2), (ALONG, 7, 1), (SEND, 9, 0), (ALONG, 3, 3), (ACROSS, 2, 3), (ACROSS, 6, 1), (ACROSS, 8, 0), (ALONG, 5, 2), (ACROSS, 4, 2), (ALONG, 8, 1), (SEND, 10, 0), (ACROSS, 7, 1), (ALONG, 4, 3), (ACROSS, 3, 3), (ACROSS, 9, 0), (ARRIVED, 1, 0),),
-    ((ALONG, 9, 1), (ALONG, 6, 2), (ACROSS, 5, 2),),
-    ((ALONG, 5, 3),),
-    ((ACROSS, 8, 1),),
-    ((ACROSS, 10, 0),),
-    ((ACROSS, 4, 3),),
-    ((ALONG, 7, 2), (ALONG, 6, 3), (ALONG, 10, 1), (ACROSS, 9, 1), (ACROSS, 6, 2), (ACROSS, 5, 3), (ALONG, 8, 2), (ARRIVED, 2, 0),),
-    ((ALONG, 7, 3), (ACROSS, 7, 2),),
-    ((ALONG, 9, 2),),
-    ((ACROSS, 6, 3), (ACROSS, 10, 1),),
-    ((ALONG, 8, 3), (ACROSS, 8, 2), (ALONG, 10, 2), (ACROSS, 7, 3), (ALONG, 9, 3), (ARRIVED, 3, 0),),
-    ((ACROSS, 9, 2), (ALONG, 10, 3),),
+    ((ALONG, 7, 3), (ALONG, 7, 2), (ACROSS, 7, 0),),
+    (),
+    ((ACROSS, 8, 2), (ACROSS, 9, 1), (ACROSS, 7, 3), (ALONG, 10, 2), (ACROSS, 10, 1), (ARRIVED, 3, 0),),
+    ((ALONG, 10, 3), (ACROSS, 7, 2), (ACROSS, 9, 2), (ACROSS, 8, 1),),
+    ((ALONG, 8, 3),),
+    ((ACROSS, 10, 2), (ACROSS, 10, 3),),
     ((ACROSS, 8, 3),),
-    ((ACROSS, 10, 2),),
-    ((ACROSS, 9, 3), (ACROSS, 10, 3),),
 )
 MIDDLES = (
-    ((ACROSS, 0, 0),),
-    ((ALONG, 0, 1), (SEND, 2, 0), (ALONG, 0, 2),),
-    ((ACROSS, 1, 0),),
+    ((ALONG, 0, 2), (SEND_ALONG, 2, 0), (SEND_ACROSS, 10, 0), (ALONG, 1, 1), (ALONG, 1, 2), (ACROSS, 10, 0),
+     (ALONG, 2, 1), (SEND_ALONG, 4, 0), (ACROSS, 0, 0), (SEND_ACROSS, 3, 0), (SEND_ALONG, 7, 0), (ALONG, 1, 3),
+     (ALONG, 2, 3), (ALONG, 0, 1), (ACROSS, 1, 1), (SEND_ACROSS, 4, 0), (SEND_ALONG, 6, 0), (ALONG, 2, 2),
+     (ACROSS, 3, 0), (ACROSS, 0, 2), (ALONG, 3, 1), (ALONG, 0, 3), (SEND_ALONG, 5, 0), (ALONG, 9, 1), (ALONG, 3, 3),
+     (SEND_ACROSS, 2, 0), (SEND_ALONG, 3, 0), (ALONG, 4, 1), (ACROSS, 2, 3), (ACROSS, 4, 0), (ALONG, 9, 3),
+     (ACROSS, 3, 1), (ALONG, 6, 1), (SEND_ACROSS, 6, 0), (ACROSS, 0, 3), (ALONG, 10, 1),),
+    ((ACROSS, 1, 2), (ALONG, 4, 2), (ACROSS, 2, 2), (ACROSS, 2, 0), (ACROSS, 1, 3), (SEND_ACROSS, 5, 0),
+     (ALONG, 6, 2), (ALONG, 4, 3), (ACROSS, 0, 1),),
+    ((ALONG, 3, 2), (SEND_ALONG, 9, 0), (ACROSS, 1, 0), (ALONG, 9, 2), (ALONG, 6, 3), (ACROSS, 2, 1), (ACROSS, 6, 0),),
+    ((ALONG, 5, 1), (ALONG, 5, 2),),
+    ((ARRIVED, 1, 0), (ACROSS, 10, 1), (SEND_ALONG, 8, 0), (ALONG, 5, 3), (ACROSS, 4, 1), (ACROSS, 4, 2),
+     (ACROSS, 4, 3), (ACROSS, 3, 2),),
     (),
-    ((ALONG, 1, 1), (SEND, 3, 0), (ALONG, 1, 2), (ACROSS, 0, 1), (ACROSS, 2, 0), (ALONG, 2, 2), (ALONG, 0, 3), (ACROSS, 0, 2), (ALONG, 2, 1), (SEND, 4, 0), (ACROSS, 1, 1), (ALONG, 3, 2), (ACROSS, 3, 0), (ALONG, 3, 1), (SEND, 5, 0), (ALONG, 1, 3), (ACROSS, 1, 2), (ACROSS, 2, 2), (ALONG, 2, 3), (ALONG, 4, 1), (SEND, 6, 0), (ALONG, 4, 2), (ACROSS, 0, 3), (ACROSS, 2, 1), (ACROSS, 4, 0), (ALONG, 5, 1), (SEND, 7, 0), (ALONG, 5, 2), (ALONG, 3, 3), (ACROSS, 3, 1), (ACROSS, 3, 2), (ACROSS, 1, 3), (ACROSS, 5, 0), (ALONG, 6, 1), (SEND, 8, 0), (ALONG, 4, 3), (ALONG, 6, 2), (ALONG, 7, 1), (SEND, 9, 0), (ALONG, 5, 3), (ACROSS, 2, 3), (ACROSS, 4, 1), (ALONG, 7, 2), (ACROSS, 4, 2), (ACROSS, 6, 0), (ALONG, 8, 1), (SEND, 10, 0), (ALONG, 6, 3), (ALONG, 8, 2), (ALONG, 9, 1), (ALONG, 7, 3), (ACROSS, 5, 1), (ACROSS, 5, 2), (ACROSS, 3, 3), (ACROSS, 7, 0), (ALONG, 9, 2), (ALONG, 8, 3), (ALONG, 10, 1), (ALONG, 9, 3), (ACROSS, 6, 1), (ALONG, 10, 2), (ARRIVED, 1, 0),),
-    ((ACROSS, 8, 0),),
-    ((ACROSS, 6, 2), (ACROSS, 4, 3),),
-    ((ALONG, 10, 3),),
     (),
-    ((ACROSS, 7, 1),),
-    ((ACROSS, 9, 0), (ACROSS, 5, 3), (ACROSS, 7, 2), (ACROSS, 8, 1), (ACROSS, 6, 3), (ACROSS, 10, 0), (ARRIVED, 2, 0),),
+    ((ALONG, 8, 1), (ACROSS, 3, 3),),
+    ((ACROSS, 6, 3), (ACROSS, 6, 1), (ALONG, 8, 2), (SEND_ACROSS, 7, 0), (ACROSS, 5, 1), (ALONG, 7, 1),
+     (SEND_ACROSS, 8, 0),),
+    ((ACROSS, 5, 2),),
+    ((ARRIVED, 2, 0), (ACROSS, 6, 2), (SEND_ALONG, 10, 0), (ALONG, 7, 3),),
+    ((ALONG, 7, 2),),
+    ((ACROSS, 8, 2), (ACROSS, 5, 0),),
+    ((SEND_ACROSS, 9, 0), (ACROSS, 5, 3), (ALONG, 10, 2), (ALONG, 10, 3),),
+    ((ACROSS, 8, 0), (ALONG, 8, 3), (ACROSS, 7, 3), (ACROSS, 7, 0), (ARRIVED, 3, 0),),
+    ((ACROSS, 9, 1), (ACROSS, 9, 3), (ACROSS, 9, 0), (ACROSS, 7, 2), (ACROSS, 7, 1), (ACROSS, 9, 2), (ACROSS, 8, 1),),
     (),
-    ((ACROSS, 8, 2),),
-    ((ACROSS, 9, 1),),
-    ((ACROSS, 7, 3), (ARRIVED, 3, 0),),
-    ((ACROSS, 9, 2), (ACROSS, 8, 3),),
-    ((ACROSS, 10, 1),),
     (),
-    ((ACROSS, 9, 3), (ACROSS, 10, 2), (ACROSS, 10, 3),),
+    ((ACROSS, 10, 2), (ACROSS, 10, 3), (ACROSS, 8, 3),),
 )
 
 
@@ -81,8 +97,8 @@
         self.index, self.weight, self.shard = index, weight, shard
         self.offset, self.rows = first * TILE, count * TILE
 
-        def share(fraction, most):
-            return TILE * min(max(round(count * fraction), least), most)
+        def share(tiles, most):
+            return TILE * min(max(round(count * tiles / UNITS[index]), least), most)
 
         self.along = share(along, count)
         self.across_own = share(across_own, count)
@@ -91,7 +107,8 @@
 
 def plain(chunks, n, seqs):
     counts = {0: seqs, 1: seqs + 2, 2: seqs, 3: seqs}
-    segments = [[(SEND, chunk.index, 0) for chunk in chunks[HEAD:]]] + [[] for _ in range(seqs)]
+    segments = [[(name, chunk.index, 0) for chunk in chunks[HEAD:] for name in (SEND_ALONG, SEND_ACROSS)]]
+    segments += [[] for _ in range(seqs)]
     for weight in range(5):
         for chunk in chunks:
             if chunk.weight == weight:
@@ -110,10 +127,10 @@
 
 def layer_kernel(n, chunks, segments, *refs):
     x_in, pool_in, out_in, up_in, gate_in, down_in = refs[:6]
-    small_in, o_ref, small = refs[6:14], refs[14], refs[15:23]
+    small_in, xm, small = refs[6:14], refs[14], refs[15:23]
     poolb, outb, upb, gateb, downb, s_pool, s_out, s_up, s_gate, s_down = refs[23:33]
-    xm, keep, sent, recv, cn, lift, ss, ssr = refs[33:41]
-    in_sem, out_sem, zs, zr, ys, yr, xs, xr, ts, tr = refs[41:]
+    keep, sent, recv, cn, lift, ss, ssr = refs[33:40]
+    in_sem, zs, zr, ys, yr, xs, xr, ts, tr = refs[40:]
     mix_gain, pool_scale, out_scale, channel_gain, up_scale, gate_scale, conv_weight, down_scale = small
     buffers = (poolb, outb, upb, gateb, downb)
 
@@ -134,18 +151,18 @@
     def order(j):
         near = jnp.minimum(a, n - 1 - a)
         odd = j % 2
-        paired = a + (1 - 2 * odd) * ((j + 1) // 2)
         way = jnp.where(a < n - 1 - a, 1, -1)
+        paired = a + way * (1 - 2 * odd) * ((j + 1) // 2)
         return jnp.where(j <= 2 * near, paired, a + way * (j - near))
 
     def rows_of(chunk, shard, start, count):
         begin = pl.multiple_of(shard * chunk.shard + chunk.offset + start, TILE)
         return buffers[chunk.weight].at[pl.ds(begin, count)]
 
-    def z_copy(chunk, s, target, slot):
+    def z_copy(chunk, s, target):
         part = rows_of(chunk, 2 * s + b, r * (chunk.rows - chunk.along), chunk.along)
         return pltpu.make_async_remote_copy(
-            src_ref=part, dst_ref=part, send_sem=zs.at[chunk.index, slot], recv_sem=zr.at[chunk.index, s],
+            src_ref=part, dst_ref=part, send_sem=zs.at[chunk.index], recv_sem=zr.at[chunk.index, s],
             device_id={"fs": 2 * target + b}, device_id_type=MESH,
         )
 
@@ -153,7 +170,7 @@
         had = chunk.across_own if own else chunk.across
         part = rows_of(chunk, 2 * s + side, r * (chunk.rows - had), had)
         return pltpu.make_async_remote_copy(
-            src_ref=part, dst_ref=part, send_sem=ys.at[chunk.index, s], recv_sem=yr.at[chunk.index, s],
+            src_ref=part, dst_ref=part, send_sem=ys.at[chunk.index], recv_sem=yr.at[chunk.index, s],
             device_id={"fs": 2 * a + 1 - b}, device_id_type=MESH,
         )
 
@@ -161,7 +178,7 @@
         had = chunk.along if kind == 0 else chunk.across_own if own else chunk.across
         part = rows_of(chunk, 2 * s + (1 - b if kind else b), end * had, chunk.rows - had)
         return pltpu.make_async_remote_copy(
-            src_ref=part, dst_ref=part, send_sem=xs.at[chunk.index, kind, s], recv_sem=xr.at[chunk.index, kind, s],
+            src_ref=part, dst_ref=part, send_sem=xs.at[chunk.index], recv_sem=xr.at[chunk.index, n * kind + s if chunk.weight == 4 else 0],
             device_id={"rep": 1 - r}, device_id_type=MESH,
         )
 
@@ -169,25 +186,26 @@
         target = jnp.where(s < a, a + 1, a - 1)
         return target, (target >= 0) & (target < n)
 
-    def begin(chunk):
+    def begin_along(chunk):
         @pl.when(a < n - 1)
         def _():
-            z_copy(chunk, a, a + 1, a).start()
+            z_copy(chunk, a, a + 1).start()
 
         @pl.when(a > 0)
         def _():
-            z_copy(chunk, a, a - 1, n).start()
-
+            z_copy(chunk, a, a - 1).start()
+
+    def begin_across(chunk):
         y_copy(chunk, a, b, True).start()
 
     def z_event(chunk, j):
         s = order(j)
         target, valid = onward(s)
-        z_copy(chunk, s, a, s).wait_recv()
+        z_copy(chunk, s, a).wait_recv()
 
         @pl.when(valid)
         def _():
-            z_copy(chunk, s, target, s).start()
+            z_copy(chunk, s, target).start()
 
         y_copy(chunk, s, b, False).start()
         if chunk.rows > chunk.along:
@@ -205,60 +223,45 @@
         if chunk.rows > had:
             x_copy(chunk, order(j), kind, 1 - r, own).wait_recv()
 
+    def bulk(chunk, sem, count):
+        part = buffers[chunk.weight].at[pl.ds(0, count)]
+        return pltpu.make_async_copy(part, part, sem)
+
+    def swapped(chunk):
+        return chunk.rows - chunk.across_own + (n - 1) * (2 * chunk.rows - chunk.along - chunk.across)
+
     def arrived(weights):
         for chunk in chunks:
-            if chunk.weight in weights:
-                x_wait(chunk, 0, 1, True)
-
-                def step(j, carry):
-                    x_wait(chunk, j, 0)
-                    x_wait(chunk, j, 1)
-                    return carry
-
-                lax.fori_loop(1, n, step, 0)
+            if chunk.weight in weights and swapped(chunk):
+                bulk(chunk, xr.at[chunk.index, 0], swapped(chunk)).wait()
+
+    inner = (a > 0) & (a < n - 1)
 
     def finish(chunk):
-        @pl.when(a < n - 1)
-        def _():
-            z_copy(chunk, a, a + 1, a).wait_send()
-
-        @pl.when(a > 0)
-        def _():
-            z_copy(chunk, a, a - 1, n).wait_send()
-
-        y_copy(chunk, a, b, True).wait_send()
-        if chunk.rows > chunk.across_own:
-            x_copy(chunk, a, 1, r, True).wait_send()
-
-        def step(j, carry):
-            s = order(j)
-            target, valid = onward(s)
-            y_copy(chunk, s, b, False).wait_send()
-            if chunk.rows > chunk.across:
-                x_copy(chunk, s, 1, r).wait_send()
-            if chunk.rows > chunk.along:
-                x_copy(chunk, s, 0, r).wait_send()
-
-            @pl.when(valid)
-            def _():
-                z_copy(chunk, s, target, s).wait_send()
-
-            return carry
-
-        lax.fori_loop(1, n, step, 0)
+        @pl.when(inner)
+        def _():
+            bulk(chunk, zs.at[chunk.index], (n + 1) * chunk.along).wait()
+
+        @pl.when(jnp.logical_not(inner))
+        def _():
+            bulk(chunk, zs.at[chunk.index], chunk.along).wait()
+
+        bulk(chunk, ys.at[chunk.index], chunk.across_own + (n - 1) * chunk.across).wait()
+        if swapped(chunk):
+            bulk(chunk, xs.at[chunk.index], swapped(chunk)).wait()
 
     def events(segment):
         for name, index, j in segment:
-            if name == SEND:
-                begin(chunks[index])
+            if name == SEND_ALONG:
+                begin_along(chunks[index])
+            elif name == SEND_ACROSS:
+                begin_across(chunks[index])
             elif name == ALONG:
                 z_event(chunks[index], j)
             elif name == ACROSS:
                 y_event(chunks[index], j)
             else:
                 arrived((0, 1) if index == 1 else (index,))
-
-    inner = (a > 0) & (a < n - 1)
 
     def between(ends, middles):
         if ends == middles:
@@ -395,20 +398,16 @@
 
     def lift_piece(q):
         cn_copy(q, 1 - core).wait_recv()
-        lift[span(q)] = (wide(q, upb) * line(up_scale)).astype(jnp.bfloat16)
-
-    def hidden_piece(q):
-        gated = wide(q, gateb) * line(gate_scale)
-        lifted = lift[span(q)].astype(jnp.float32)
+        lifted = (wide(q, upb) * line(up_scale)).astype(jnp.bfloat16).astype(jnp.float32)
         at = lax.broadcasted_iota(jnp.int32, (LENGTH, 1), 0)
         before = jnp.where(at == 0, 0.0, pltpu.roll(lifted, 1, 0))
         after = jnp.where(at == LENGTH - 1, 0.0, pltpu.roll(lifted, LENGTH - 1, 0))
-        conv = (
-            conv_weight[0:1, :] * before
-            + conv_weight[1:2, :] * lifted
-            + conv_weight[2:3, :] * after
-        )
-        lift[span(q)] = (jax.nn.gelu(conv) * gated).astype(jnp.bfloat16)
+        conv = conv_weight[0:1, :] * before + conv_weight[1:2, :] * lifted + conv_weight[2:3, :] * after
+        lift[span(q)] = jax.nn.gelu(conv).astype(jnp.bfloat16)
+
+    def hidden_piece(q):
+        gated = wide(q, gateb) * line(gate_scale)
+        lift[span(q)] = (lift[span(q)].astype(jnp.float32) * gated).astype(jnp.bfloat16)
 
     loads = [
         pltpu.make_async_copy(out_in, s_out, in_sem.at[0]),
@@ -443,7 +442,8 @@
     pl.semaphore_wait(barrier, 3 + ends)
 
     for chunk in chunks[:HEAD]:
-        begin(chunk)
+        begin_along(chunk)
+        begin_across(chunk)
     settle(3, s_up, upb)
     for load in loads[2:3] + loads[6:]:
         load.wait()
@@ -469,7 +469,7 @@
     stage(3 + 3 * seqs, seqs, hidden_piece)
     down_c = [chunk for chunk in chunks if chunk.weight == 4]
     for chunk in chunks:
-        if chunk.weight < 3:
+        if chunk.weight < 4:
             finish(chunk)
 
     shard_rows = s_down.shape[0]
@@ -517,25 +517,19 @@
 
     lax.fori_loop(0, blocks, down_wait, 0)
 
-    def result(q):
-        return pltpu.make_async_copy(xm.at[span(q)], o_ref.at[span(q)], out_sem.at[q])
-
     def last(q, carry):
         xm[span(q)] = (xm[span(q)].astype(jnp.float32) + both(q) * line(down_scale)).astype(jnp.bfloat16)
-        result(q).start()
         return carry
 
     lax.fori_loop(0, seqs, last, 0)
 
-    for chunk in chunks:
-        if chunk.weight >= 3:
-            finish(chunk)
+    for chunk in down_c:
+        finish(chunk)
 
     def sends(q, carry):
         norm_copy(0, q).wait_send()
         norm_copy(1, q).wait_send()
         cn_copy(q, core).wait_send()
-        result(q).wait()
         return carry
 
     lax.fori_loop(0, seqs, sends, 0)
@@ -590,9 +584,9 @@
     dma = pltpu.SemaphoreType.DMA
     return pl.pallas_call(
         functools.partial(layer_kernel, n, chunks, segments),
-        out_shape=jax.ShapeDtypeStruct((rows, half), bf16),
+        out_shape=pltpu.VMEM((rows, half), bf16),
         in_specs=[pl.BlockSpec(memory_space=pl.ANY)] * (6 + len(small)),
-        out_specs=pl.BlockSpec(memory_space=pl.ANY),
+        out_specs=pl.BlockSpec(memory_space=pltpu.VMEM),
         scratch_shapes=[pltpu.VMEM(v.shape, v.dtype) for v in small]
         + [
             pltpu.VMEM((shards * groups * lane, group), bf16),
@@ -605,7 +599,6 @@
             pltpu.VMEM(up_weight.shape, f32),
             pltpu.VMEM(gate_weight.shape, f32),
             pltpu.VMEM(down_weight.shape, f32),
-            pltpu.VMEM((rows, half), bf16),
             pltpu.VMEM((blocks, rows, block), bf16),
             pltpu.VMEM((blocks, rows, block), bf16),
             pltpu.VMEM((blocks, rows, block), bf16),
@@ -614,18 +607,17 @@
             pltpu.VMEM((2, rows, 128), f32),
             pltpu.VMEM((2, rows, 128), f32),
             dma((6 + len(small),)),
-            dma((seqs,)),
-            dma((count, n + 1)),
+            dma((count,)),
             dma((count, n)),
+            dma((count,)),
             dma((count, n)),
-            dma((count, n)),
-            dma((count, 2, n)),
-            dma((count, 2, n)),
+            dma((count,)),
+            dma((count, 2 * n)),
             dma((5, max(seqs, blocks))),
             dma((5, max(seqs, blocks))),
         ],
         compiler_params=pltpu.CompilerParams(
-            collective_id=0, has_side_effects=True, vmem_limit_bytes=67_043_328
+            collective_id=0, has_side_effects=True, vmem_limit_bytes=62_000_000
         ),
         name="layer",
     )(layer_in, pool_rows, out_weight, up_weight, gate_weight, down_weight, *small)

time: 168 us -> 163 us (0.970)
  Pallas kernels: 165 us -> 162 us
  local copies, waits for them, and re-layouts: 3.08 us -> 1.32 us
    pallas_call x1, Pallas kernels: 165 us -> 162 us  [per_device(): pl.pallas_call(functools.partial(layer_kernel, n, chunks, segments), out_...]
    unnamed x1, local copies, waits for them, and re-layouts: 3.08 us -> 1.32 us
where the time goes in v2:
time: 163 us
  Pallas kernels  162 us (99%)
    pallas_call x1, Pallas kernels, per_device(): pl.pallas_call(functools.partial(layer_kernel, n, chunks, segments), out_...  162 us

profile of v2, /device:TPU:1, one launch (start us, length us, event | category | flops | bytes accessed | tf_op | source)
XLA Modules:
  0.0 163.0 jit_solution(17398173417718542773)
XLA Ops:
  0.0 161.7 %layer.1 = bf16[1024,1024]{1,0:T(8,128)(2,1)S(1)} custom-call(bf16[1024,1024]{1,0:T(8,128)(2,1)} %refs_0_.1, f32[128,512]{1,0:T(8,128)} %bitcast.5, f32[1024,256]{1,0:T(8,128)} %refs_2_.1, f32[256,1408]{1,0:T(8,128)} %refs_3_.1, f32[256,1408]{1,0:T(8,128)} %refs_4_.1, f32[1408,256]{1,0:T(8,128)} %refs_5_.1, bf16[1024]{0:T(1024)(128)(2,1)} %refs_6_.1, ...), custom_call_target="tpu_custom_call" | custom-call | tf_op jit(solution)/shard_map/layer/pallas_call | solution.py:585
  161.7 1.3 copy.16

commit v3 on v2

--- a/solution.py
+++ b/solution.py
@@ -13,92 +13,107 @@
 MESH = pl.DeviceIdType.MESH
 
 PLAN = (
-    (0, 0, 1, 4, 5, 4),
-    (1, 0, 2, 16, 17, 16),
-    (1, 1, 2, 17, 16, 16),
-    (2, 0, 2, 4, 4, 4),
-    (2, 1, 2, 6, 4, 4),
-    (3, 0, 2, 8, 8, 5),
-    (3, 1, 2, 7, 4, 6),
-    (4, 0, 4, 20, 11, 17),
-    (4, 1, 4, 19, 11, 14),
-    (4, 2, 4, 20, 19, 11),
-    (4, 3, 4, 22, 17, 12),
+    (0, 0, 8, 4, 4, 4),
+    (1, 0, 32, 17, 16, 17),
+    (1, 32, 64, 19, 20, 17),
+    (2, 0, 8, 4, 4, 4),
+    (2, 8, 16, 4, 6, 4),
+    (3, 0, 8, 8, 4, 7),
+    (3, 8, 16, 8, 5, 4),
+    (4, 0, 22, 22, 12, 15),
+    (4, 22, 44, 21, 14, 11),
+    (4, 44, 66, 21, 11, 12),
+    (4, 66, 88, 22, 16, 22),
 )
-UNITS = (8, 32, 32, 8, 8, 8, 8, 22, 22, 22, 22)
+UNITS = (8, 64, 16, 16, 88)
 HEAD = 2
 SEND_ALONG, SEND_ACROSS, ALONG, ACROSS, ARRIVED = range(5)
 
 ENDS = (
-    ((SEND_ACROSS, 4, 0), (SEND_ALONG, 2, 0), (SEND_ALONG, 3, 0), (ALONG, 0, 1), (SEND_ALONG, 9, 0), (ALONG, 1, 1),
-     (ALONG, 0, 2), (ACROSS, 1, 0),),
-    ((ALONG, 2, 1), (SEND_ALONG, 6, 0), (ALONG, 1, 2), (SEND_ACROSS, 3, 0), (SEND_ACROSS, 2, 0), (ACROSS, 4, 0),
-     (ACROSS, 1, 1), (SEND_ACROSS, 9, 0), (ACROSS, 1, 2), (ALONG, 1, 3), (SEND_ALONG, 4, 0), (ALONG, 4, 1),
-     (SEND_ALONG, 10, 0), (ALONG, 2, 3), (SEND_ACROSS, 8, 0), (ACROSS, 2, 1), (ACROSS, 1, 3), (ALONG, 2, 2),
-     (SEND_ACROSS, 6, 0), (ACROSS, 0, 1),),
-    ((ACROSS, 2, 0), (ACROSS, 0, 0), (ALONG, 7, 1), (ACROSS, 3, 0), (ACROSS, 2, 3), (ALONG, 0, 3), (ALONG, 3, 3),
-     (SEND_ACROSS, 10, 0),),
-    ((SEND_ACROSS, 5, 0), (ALONG, 3, 1), (ALONG, 6, 1), (ACROSS, 2, 2), (SEND_ALONG, 8, 0), (ACROSS, 0, 2),
-     (ACROSS, 10, 0), (ACROSS, 0, 3), (ACROSS, 5, 0), (ACROSS, 6, 0), (ACROSS, 8, 0),),
-    ((SEND_ALONG, 5, 0), (ALONG, 9, 3), (SEND_ACROSS, 7, 0), (ALONG, 5, 1), (ACROSS, 4, 1), (ACROSS, 6, 1),
-     (ALONG, 4, 2), (ARRIVED, 1, 0), (SEND_ALONG, 7, 0),),
-    ((ACROSS, 3, 3), (ALONG, 4, 3), (ALONG, 3, 2),),
-    ((ACROSS, 5, 1), (ALONG, 6, 3), (ACROSS, 4, 3), (ACROSS, 7, 1),),
-    ((ACROSS, 3, 1), (ALONG, 6, 2), (ALONG, 9, 2), (ACROSS, 3, 2), (ALONG, 5, 2),),
-    ((ACROSS, 4, 2), (ACROSS, 6, 2), (ACROSS, 9, 3), (ACROSS, 6, 3), (ALONG, 5, 3), (ALONG, 8, 1),),
-    ((ACROSS, 9, 0),),
-    ((ARRIVED, 2, 0), (ACROSS, 5, 3), (ACROSS, 5, 2), (ALONG, 9, 1), (ALONG, 8, 2), (ALONG, 10, 1),),
-    (),
-    ((ALONG, 7, 3), (ALONG, 7, 2), (ACROSS, 7, 0),),
-    (),
-    ((ACROSS, 8, 2), (ACROSS, 9, 1), (ACROSS, 7, 3), (ALONG, 10, 2), (ACROSS, 10, 1), (ARRIVED, 3, 0),),
-    ((ALONG, 10, 3), (ACROSS, 7, 2), (ACROSS, 9, 2), (ACROSS, 8, 1),),
-    ((ALONG, 8, 3),),
-    ((ACROSS, 10, 2), (ACROSS, 10, 3),),
-    ((ACROSS, 8, 3),),
+    ((SEND_ALONG, 10, 0), (SEND_ACROSS, 3, 0), (ALONG, 0, 1), (ACROSS, 0, 0), (SEND_ACROSS, 8, 0),),
+    ((ACROSS, 1, 0), (ALONG, 1, 1), (SEND_ALONG, 2, 0),),
+    ((ALONG, 2, 1), (ACROSS, 3, 0), (SEND_ACROSS, 2, 0), (SEND_ALONG, 4, 0), (ALONG, 4, 1), (SEND_ALONG, 3, 0),
+     (ALONG, 1, 2), (SEND_ALONG, 9, 0), (ACROSS, 0, 1), (ALONG, 3, 1), (ACROSS, 1, 1), (ALONG, 0, 3),
+     (SEND_ALONG, 6, 0), (ACROSS, 2, 1), (SEND_ALONG, 7, 0), (ALONG, 0, 2), (ACROSS, 1, 2),),
+    ((ACROSS, 4, 1), (SEND_ACROSS, 7, 0), (ACROSS, 0, 3), (ALONG, 2, 3), (SEND_ALONG, 8, 0), (SEND_ALONG, 5, 0),
+     (ACROSS, 2, 0), (SEND_ACROSS, 5, 0),),
+    ((ALONG, 2, 2), (ACROSS, 5, 0), (ACROSS, 3, 1), (ACROSS, 2, 3), (SEND_ACROSS, 9, 0), (SEND_ACROSS, 4, 0),
+     (ALONG, 4, 3), (ALONG, 3, 3), (ALONG, 1, 3), (ALONG, 4, 2), (ACROSS, 0, 2), (SEND_ACROSS, 6, 0), (ACROSS, 1, 3),
+     (ACROSS, 4, 0), (ACROSS, 2, 2), (ALONG, 3, 2), (ALONG, 5, 1), (ACROSS, 9, 0), (ACROSS, 3, 2), (ALONG, 6, 1),
+     (ACROSS, 5, 1), (SEND_ACROSS, 10, 0), (ARRIVED, 1, 0), (ALONG, 6, 3), (ALONG, 9, 1), (ACROSS, 4, 3),),
+    ((ALONG, 6, 2), (ALONG, 8, 1), (ALONG, 5, 3), (ACROSS, 6, 1), (ACROSS, 4, 2), (ACROSS, 3, 3),),
+    (),
+    ((ALONG, 5, 2),),
+    ((ACROSS, 6, 2),),
+    ((ALONG, 7, 1), (ACROSS, 6, 0),),
+    ((ACROSS, 6, 3), (ALONG, 9, 2), (ARRIVED, 2, 0),),
+    (),
+    ((ACROSS, 5, 2), (ALONG, 10, 1),),
+    ((ALONG, 8, 3), (ACROSS, 5, 3), (ACROSS, 9, 2), (ACROSS, 8, 1), (ACROSS, 7, 0), (ACROSS, 8, 0), (ALONG, 8, 2),),
+    ((ACROSS, 7, 1), (ACROSS, 10, 0), (ALONG, 7, 2), (ARRIVED, 3, 0),),
+    ((ALONG, 9, 3), (ACROSS, 9, 1),),
+    (),
+    ((ACROSS, 8, 3), (ACROSS, 10, 1), (ACROSS, 8, 2), (ALONG, 10, 2),),
+    ((ACROSS, 7, 2), (ALONG, 7, 3),),
+    (),
+    (),
+    ((ACROSS, 10, 2), (ALONG, 10, 3), (ACROSS, 9, 3),),
+    ((ACROSS, 7, 3),),
+    (),
+    (),
+    ((ACROSS, 10, 3),),
+    (),
 )
 MIDDLES = (
-    ((ALONG, 0, 2), (SEND_ALONG, 2, 0), (SEND_ACROSS, 10, 0), (ALONG, 1, 1), (ALONG, 1, 2), (ACROSS, 10, 0),
-     (ALONG, 2, 1), (SEND_ALONG, 4, 0), (ACROSS, 0, 0), (SEND_ACROSS, 3, 0), (SEND_ALONG, 7, 0), (ALONG, 1, 3),
-     (ALONG, 2, 3), (ALONG, 0, 1), (ACROSS, 1, 1), (SEND_ACROSS, 4, 0), (SEND_ALONG, 6, 0), (ALONG, 2, 2),
-     (ACROSS, 3, 0), (ACROSS, 0, 2), (ALONG, 3, 1), (ALONG, 0, 3), (SEND_ALONG, 5, 0), (ALONG, 9, 1), (ALONG, 3, 3),
-     (SEND_ACROSS, 2, 0), (SEND_ALONG, 3, 0), (ALONG, 4, 1), (ACROSS, 2, 3), (ACROSS, 4, 0), (ALONG, 9, 3),
-     (ACROSS, 3, 1), (ALONG, 6, 1), (SEND_ACROSS, 6, 0), (ACROSS, 0, 3), (ALONG, 10, 1),),
-    ((ACROSS, 1, 2), (ALONG, 4, 2), (ACROSS, 2, 2), (ACROSS, 2, 0), (ACROSS, 1, 3), (SEND_ACROSS, 5, 0),
-     (ALONG, 6, 2), (ALONG, 4, 3), (ACROSS, 0, 1),),
-    ((ALONG, 3, 2), (SEND_ALONG, 9, 0), (ACROSS, 1, 0), (ALONG, 9, 2), (ALONG, 6, 3), (ACROSS, 2, 1), (ACROSS, 6, 0),),
-    ((ALONG, 5, 1), (ALONG, 5, 2),),
-    ((ARRIVED, 1, 0), (ACROSS, 10, 1), (SEND_ALONG, 8, 0), (ALONG, 5, 3), (ACROSS, 4, 1), (ACROSS, 4, 2),
-     (ACROSS, 4, 3), (ACROSS, 3, 2),),
-    (),
-    (),
-    ((ALONG, 8, 1), (ACROSS, 3, 3),),
-    ((ACROSS, 6, 3), (ACROSS, 6, 1), (ALONG, 8, 2), (SEND_ACROSS, 7, 0), (ACROSS, 5, 1), (ALONG, 7, 1),
-     (SEND_ACROSS, 8, 0),),
-    ((ACROSS, 5, 2),),
-    ((ARRIVED, 2, 0), (ACROSS, 6, 2), (SEND_ALONG, 10, 0), (ALONG, 7, 3),),
-    ((ALONG, 7, 2),),
-    ((ACROSS, 8, 2), (ACROSS, 5, 0),),
-    ((SEND_ACROSS, 9, 0), (ACROSS, 5, 3), (ALONG, 10, 2), (ALONG, 10, 3),),
-    ((ACROSS, 8, 0), (ALONG, 8, 3), (ACROSS, 7, 3), (ACROSS, 7, 0), (ARRIVED, 3, 0),),
-    ((ACROSS, 9, 1), (ACROSS, 9, 3), (ACROSS, 9, 0), (ACROSS, 7, 2), (ACROSS, 7, 1), (ACROSS, 9, 2), (ACROSS, 8, 1),),
-    (),
-    (),
-    ((ACROSS, 10, 2), (ACROSS, 10, 3), (ACROSS, 8, 3),),
+    ((SEND_ALONG, 2, 0), (SEND_ALONG, 4, 0), (ACROSS, 0, 0), (ALONG, 0, 1), (ALONG, 0, 2), (ALONG, 1, 2),
+     (SEND_ACROSS, 9, 0), (SEND_ALONG, 3, 0), (ACROSS, 1, 0),),
+    ((ALONG, 1, 1), (ALONG, 2, 1), (ALONG, 4, 1), (ACROSS, 1, 1), (SEND_ALONG, 8, 0), (ALONG, 0, 3), (ALONG, 1, 3),
+     (ALONG, 2, 2), (ACROSS, 2, 1), (ALONG, 2, 3), (ALONG, 3, 2), (ALONG, 3, 1), (SEND_ALONG, 7, 0), (ALONG, 6, 1),
+     (SEND_ACROSS, 6, 0), (ACROSS, 0, 1), (SEND_ACROSS, 8, 0), (ALONG, 3, 3), (ALONG, 4, 3), (ACROSS, 2, 2),
+     (ALONG, 4, 2), (ACROSS, 6, 0), (SEND_ALONG, 5, 0), (SEND_ACROSS, 2, 0), (ACROSS, 6, 1), (ALONG, 5, 1),
+     (ACROSS, 2, 3), (SEND_ACROSS, 5, 0), (SEND_ACROSS, 3, 0), (ALONG, 6, 3), (SEND_ALONG, 6, 0),),
+    (),
+    ((ACROSS, 0, 2), (ACROSS, 0, 3), (ACROSS, 1, 3), (ACROSS, 4, 3), (ALONG, 9, 1), (SEND_ALONG, 9, 0),
+     (SEND_ACROSS, 4, 0), (ACROSS, 4, 1), (ACROSS, 2, 0), (SEND_ACROSS, 7, 0),),
+    ((ALONG, 6, 2), (ACROSS, 1, 2), (ACROSS, 3, 3), (ACROSS, 5, 0), (ALONG, 5, 3), (SEND_ACROSS, 10, 0),
+     (ALONG, 5, 2), (ALONG, 10, 1), (ARRIVED, 1, 0), (ACROSS, 3, 1), (ACROSS, 3, 2), (ACROSS, 3, 0), (ACROSS, 4, 2),),
+    (),
+    ((ALONG, 8, 2),),
+    ((ALONG, 8, 1),),
+    ((ACROSS, 4, 0), (ACROSS, 6, 3), (ALONG, 9, 2),),
+    ((SEND_ALONG, 10, 0), (ALONG, 7, 1),),
+    ((ALONG, 8, 3), (ACROSS, 5, 1), (ACROSS, 5, 2), (ARRIVED, 2, 0), (ACROSS, 6, 2), (ACROSS, 10, 0), (ALONG, 7, 2),
+     (ALONG, 9, 3), (ACROSS, 9, 0), (ALONG, 10, 2),),
+    ((ACROSS, 5, 3), (ACROSS, 7, 0),),
+    (),
+    ((ACROSS, 8, 1),),
+    ((ACROSS, 9, 1), (ALONG, 7, 3), (ARRIVED, 3, 0), (ACROSS, 8, 0),),
+    ((ACROSS, 7, 1),),
+    ((ACROSS, 8, 2), (ACROSS, 9, 2), (ALONG, 10, 3),),
+    (),
+    ((ACROSS, 8, 3), (ACROSS, 10, 1),),
+    ((ACROSS, 7, 2), (ACROSS, 9, 3),),
+    (),
+    (),
+    ((ACROSS, 7, 3), (ACROSS, 10, 2),),
+    (),
+    (),
+    ((ACROSS, 10, 3),),
+    (),
 )
 
 
 class Chunk:
-    def __init__(self, index, weight, shard, part, parts, along, across_own, across):
-        units = shard // TILE
-        first, last = units * part // parts, units * (part + 1) // parts
-        count = last - first
+    def __init__(self, index, weight, shard, first, last, along, across_own, across):
+        tiles = shard // TILE
+        begin, end = tiles * first // UNITS[weight], tiles * last // UNITS[weight]
+        count = end - begin
         least = (count + 1) // 2
         self.index, self.weight, self.shard = index, weight, shard
-        self.offset, self.rows = first * TILE, count * TILE
-
-        def share(tiles, most):
-            return TILE * min(max(round(count * tiles / UNITS[index]), least), most)
+        self.offset, self.rows = begin * TILE, count * TILE
+
+        def share(part, most):
+            return TILE * min(max(round(count * part / (last - first)), least), most)
 
         self.along = share(along, count)
         self.across_own = share(across_own, count)
@@ -280,7 +295,7 @@
         def step(q, carry):
             piece(q)
             for i in range(count):
-                if segments[0][first + i] or segments[1][first + i]:
+                if first + i < len(segments[0]) and (segments[0][first + i] or segments[1][first + i]):
 
                     @pl.when(q == i)
                     def _(i=i):
@@ -468,60 +483,73 @@
     stage(3 + 2 * seqs, seqs, lift_piece)
     stage(3 + 3 * seqs, seqs, hidden_piece)
     down_c = [chunk for chunk in chunks if chunk.weight == 4]
-    for chunk in chunks:
-        if chunk.weight < 4:
-            finish(chunk)
-
     shard_rows = s_down.shape[0]
 
-    def down_step(i, carry):
+    def place(i):
+        shard = 2 * order(i // 2) + (b + i) % 2
+        return shard, shard // blocks, shard % blocks
+
+    def settle_block(i):
+        _, side, index = place(i)
+        for k in range(blocks):
+
+            @pl.when((side == core) & (index == k))
+            def _(k=k):
+                down_copy(k).wait_recv()
+                columns = slice(k * block, (k + 1) * block)
+                scale = down_scale[:, columns]
+
+                def part(q, carry):
+                    added = keep[k, span(q)].astype(jnp.float32) + recv[k, span(q)].astype(jnp.float32)
+                    xm[span(q), columns] = (xm[span(q), columns].astype(jnp.float32) + added * scale).astype(jnp.bfloat16)
+                    return carry
+
+                lax.fori_loop(0, seqs, part, 0)
+
+    def down_step(i):
         j, kind = i // 2, i % 2
-        s = order(j)
+
+        @pl.when(i >= 2)
+        def _():
+            settle_block(i - 2)
 
         @pl.when((kind == 1) & (j == 0))
         def _():
             for chunk in down_c:
                 x_wait(chunk, 0, 1, True)
 
-        @pl.when((kind == 1) & (j > 0))
+        @pl.when((kind == 1) & (j > 0) & (j < n))
         def _():
             for chunk in down_c:
                 x_wait(chunk, j, 1)
 
-        @pl.when((kind == 0) & (j > 0))
+        @pl.when((kind == 0) & (j > 0) & (j < n))
         def _():
             for chunk in down_c:
                 x_wait(chunk, j, 0)
 
-        shard = 2 * s + (b + kind) % 2
-        start = pl.multiple_of(shard * shard_rows, TILE)
-        side, index = shard // blocks, shard % blocks
-        product = dot(lift[...], downb[pl.ds(start, shard_rows), :]).astype(jnp.bfloat16)
-
-        @pl.when(side == core)
-        def _():
-            keep[index] = product
-
-        @pl.when(side != core)
-        def _():
-            sent[index] = product
-            down_copy(index).start()
-
-        return carry
-
-    lax.fori_loop(0, shards, down_step, 0)
-
-    def down_wait(index, carry):
-        down_copy(index).wait_recv()
-        return carry
-
-    lax.fori_loop(0, blocks, down_wait, 0)
-
-    def last(q, carry):
-        xm[span(q)] = (xm[span(q)].astype(jnp.float32) + both(q) * line(down_scale)).astype(jnp.bfloat16)
-        return carry
-
-    lax.fori_loop(0, seqs, last, 0)
+        @pl.when(j < n)
+        def _():
+            shard, side, index = place(i)
+            start = pl.multiple_of(shard * shard_rows, TILE)
+            product = dot(lift[...], downb[pl.ds(start, shard_rows), :]).astype(jnp.bfloat16)
+
+            @pl.when(side == core)
+            def _():
+                keep[index] = product
+
+            @pl.when(side != core)
+            def _():
+                sent[index] = product
+                down_copy(index).start()
+
+        @pl.when(i == shards)
+        def _():
+            for chunk in chunks:
+                if chunk.weight < 4:
+                    finish(chunk)
+
+    stage(3 + 4 * seqs, shards + 2, down_step)
 
     for chunk in down_c:
         finish(chunk)

time: 163 us -> 157 us (0.963)
  Pallas kernels: 162 us -> 156 us
    pallas_call x1, Pallas kernels: 162 us -> 156 us  [per_device(): pl.pallas_call(functools.partial(layer_kernel, n, chunks, segments), out_...]
where the time goes in v3:
time: 157 us
  Pallas kernels  156 us (99%)
    pallas_call x1, Pallas kernels, per_device(): pl.pallas_call(functools.partial(layer_kernel, n, chunks, segments), out_...  156 us

profile of v3, /device:TPU:1, one launch (start us, length us, event | category | flops | bytes accessed | tf_op | source)
XLA Modules:
  0.0 157.3 jit_solution(17622929800438024071)
XLA Ops:
  0.0 156.0 %layer.1 = bf16[1024,1024]{1,0:T(8,128)(2,1)S(1)} custom-call(bf16[1024,1024]{1,0:T(8,128)(2,1)} %refs_0_.1, f32[128,512]{1,0:T(8,128)} %bitcast.5, f32[1024,256]{1,0:T(8,128)} %refs_2_.1, f32[256,1408]{1,0:T(8,128)} %refs_3_.1, f32[256,1408]{1,0:T(8,128)} %refs_4_.1, f32[1408,256]{1,0:T(8,128)} %refs_5_.1, bf16[1024]{0:T(1024)(128)(2,1)} %refs_6_.1, ...), custom_call_target="tpu_custom_call" | custom-call | tf_op jit(solution)/shard_map/layer/pallas_call | solution.py:613
  156.0 1.3 copy.16
